TPU v7x, 512 devices: a whole 4x4x16 slice. The times are simulated.
512 devices in a mesh: ep: 128 (over z, x, core), tp: 4 (over y).
Axes of the slice: x: 4, y: 4, z: 16, core: 2. Of those that a mesh axis runs over, the one named last changes fastest.
Arguments:
- tokens: bfloat16 [16384, 4096], P('ep', 'tp'), may hold values from -6 to 6
- norm_gain: float32 [4096], replicated, may hold values from 0.1 to 1.9
- expert_ids: int32 [16384, 2], P('ep'), may hold values from 0 to 127, all different within a row; in each aligned block of 128 rows (0 to 127, 128 to 255, ...) at most 3 rows name the same one
- expert_gates: float32 [16384, 2], P('ep'), may hold values from 0.2 to 1
- gate_proj: bfloat16 [128, 4096, 512], P('ep', None, 'tp'), may hold values from -0.09375 to 0.09375
- up_proj: bfloat16 [128, 4096, 512], P('ep', None, 'tp'), may hold values from -0.09375 to 0.09375
- down_proj: bfloat16 [128, 512, 4096], P('ep', None, 'tp'), may hold values from -0.25 to 0.25
- shared_gate: bfloat16 [4096, 512], P('ep', 'tp'), may hold values from -0.09375 to 0.09375
- shared_up: bfloat16 [4096, 512], P('ep', 'tp'), may hold values from -0.09375 to 0.09375
- shared_down: bfloat16 [512, 4096], P(None, 'tp'), may hold values from -0.25 to 0.25
Outputs:
- mixed: bfloat16 [16384, 4096], P('ep', 'tp')
Inputs may be any that keep to these rules, and one draw needn't show every extreme that they name: `expert_ids`: each row names 2 distinct experts. Among the 128 rows of one index of ep (aligned blocks) no expert is named by more than 3 rows, a bound that some block reaches.
All inputs are finite; a program needn't handle non-finite values.
Results may differ from a plain program's by a relative error of at most 0.0067.
Values may be sent and summed in bfloat16 or wider, within the bound.
A program may use at most 64 MiB of HBM per device.

v0:
```python
import jax
import jax.numpy as jnp
from jax import lax
from jax.sharding import Mesh
from jax.sharding import PartitionSpec as P

EP = ("ep_0", "ep_1", "ep_2")


def copy_for_each(value, axis):
    peers = lax.axis_size(axis)
    return lax.all_to_all(
        jnp.broadcast_to(value[None], (peers, *value.shape)), axis, 0, 0, tiled=True
    )


def laid_out(blocks, dim):
    shape = list(blocks.shape[1:])
    shape[dim] *= blocks.shape[0]
    return jnp.moveaxis(blocks, 0, dim).reshape(shape)


def collect(value, axis, dim):
    blocks = copy_for_each(value, axis)
    return laid_out(blocks, dim)


def sent_together(arrays, axis, dim, along):
    both = jnp.concatenate(arrays, axis=along)
    filled, at, outs = (lax.all_gather(both, axis, axis=dim, tiled=True), 0, [])
    for a in arrays:
        outs.append(lax.slice_in_dim(filled, at, at + a.shape[along], axis=along))
        at += a.shape[along]
    return tuple(outs)


def split_up(value, dim, peers):
    before, after = (value.shape[:dim], value.shape[dim + 1 :])
    return jnp.moveaxis(value.reshape(*before, peers, -1, *after), dim, 0)


def turned_blocks(blocks, axes, sequence):
    inside = blocks.shape[1:]
    filled = blocks.reshape(*(lax.axis_size(a) for a in axes), *inside)
    for k in sequence:
        filled = lax.all_to_all(filled, axes[k], k, k, tiled=True)
    return filled.reshape(-1, *inside)


def core_and_chips(value, groups, sequence, split_dim, concat_dim):
    peers = lax.axis_size(groups[0]) * lax.axis_size(groups[1])
    blocks = split_up(value, split_dim, peers)
    return laid_out(turned_blocks(blocks, groups, sequence), concat_dim)


def shards(
    tokens,
    norm_gain,
    expert_ids,
    expert_gates,
    gate_proj,
    up_proj,
    down_proj,
    shared_gate,
    shared_up,
    shared_down,
):
    n_ep = lax.axis_size(EP)
    n_tp = lax.axis_size("tp")
    whole = collect(tokens, "tp", 1)
    tok_rows, width = whole.shape
    quarter = width // n_tp
    floats = whole.astype(jnp.float32)
    scale = lax.rsqrt(jnp.mean(floats * floats, axis=-1, keepdims=True) + 1e-06)
    normed = (floats * scale * norm_gain[None, :]).astype(jnp.bfloat16)
    gate_whole, up_whole = sent_together((shared_gate, shared_up), EP, 0, 1)
    shared_g = jnp.dot(normed, gate_whole, preferred_element_type=jnp.float32)
    shared_u = jnp.dot(normed, up_whole, preferred_element_type=jnp.float32)
    shared_hidden = (jax.nn.silu(shared_g) * shared_u).astype(jnp.bfloat16)
    rows = shared_down
    shared_out = jnp.dot(collect(shared_hidden, "tp", 1), rows, preferred_element_type=jnp.float32)
    exp_dev = gate_proj.shape[0]
    n_exp = exp_dev * n_ep
    top = expert_ids.shape[1]
    cap = 3 * tok_rows * top // (2 * n_exp)
    flat_ids = expert_ids.reshape(tok_rows * top)
    onehot = (flat_ids[:, None] == jnp.arange(n_exp, dtype=jnp.int32)[None, :]).astype(jnp.int32)
    slots = jnp.sum((jnp.cumsum(onehot, axis=0) - onehot) * onehot, axis=-1)
    dest = flat_ids * cap + slots
    local_tok = jnp.repeat(jnp.arange(tok_rows, dtype=jnp.int32), top)
    owner = jnp.full((n_exp * cap,), tok_rows, jnp.int32).at[dest].set(local_tok)
    own_part = lax.dynamic_slice_in_dim(normed, lax.axis_index("tp") * quarter, quarter, 1)
    padded = jnp.concatenate([own_part, jnp.zeros((1, quarter), jnp.bfloat16)], axis=0)
    outgoing = padded[owner].reshape(n_ep, exp_dev, cap, quarter)
    arrived = core_and_chips(outgoing, (("ep_0", "ep_1"), "ep_2"), (1, 0), 0, 0)
    received = collect(arrived, "tp", 3)
    gate_vals = jnp.einsum(
        "secd,edh->sech", received, gate_proj, preferred_element_type=jnp.float32
    )
    up_vals = jnp.einsum("secd,edh->sech", received, up_proj, preferred_element_type=jnp.float32)
    expert_hidden = (jax.nn.silu(gate_vals) * up_vals).astype(jnp.bfloat16)
    rows = down_proj
    expert_out = jnp.einsum(
        "sech,ehd->secd", collect(expert_hidden, "tp", 3), rows, preferred_element_type=jnp.float32
    ).astype(jnp.bfloat16)
    returned = lax.all_to_all(expert_out, EP, split_axis=0, concat_axis=0, tiled=True)
    picked = returned.reshape(n_exp * cap, quarter)[dest].reshape(tok_rows, top, quarter)
    routed = jnp.sum(expert_gates[:, :, None] * picked.astype(jnp.float32), axis=1)
    return (routed + shared_out).astype(jnp.bfloat16)


def solution(mesh):
    finer = Mesh(mesh.devices.reshape(16, 4, 2, mesh.shape["tp"]), ("ep_0", "ep_1", "ep_2", "tp"))
    in_specs = (
        P(EP, "tp"),
        P(),
        P(EP, None),
        P(EP, None),
        P(EP, None, "tp"),
        P(EP, None, "tp"),
        P(EP, None, "tp"),
        P(EP, "tp"),
        P(EP, "tp"),
        P(None, "tp"),
    )
    out_specs = P(EP, "tp")
    return jax.shard_map(
        shards, mesh=finer, in_specs=in_specs, out_specs=out_specs, check_vma=False
    )
```

profile of v0, /device:TPU:1, one launch (start us, length us, event | category | flops | bytes accessed | tf_op | source)
XLA Modules:
  0.0 273.0 jit_solution(16409234767689712165)
XLA Ops:
  6.5 2.2 broadcast_in_dim.18
  8.7 5.0 %all-to-all-start = ((bf16[4,128,1024]{2,1,0:T(8,128)(2,1)}), bf16[4,128,1024]{2,1,0:T(8,128)(2,1)S(1)}, u32[]{:S(2)}, u32[]{:S(2)}) async-start(bf16[4,128,1024]{2,1,0:T(8,128)(2,1)} %broadcast_in_dim.18), calls=%async_computation | async-start | bytes 2097152 | tf_op jit(solution)/shard_map/all_to_all | solution.py:12
  13.7 0.1 copy.38
  13.8 0.1 eq.29
  13.9 0.1 copy.40
  14.1 0.2 fusion.13
  14.4 0.1 eq.25
  14.5 0.1 copy.37
  14.6 0.1 mul.74
  14.8 0.1 reshape.135
  14.9 0.2 fusion.15
  15.1 1.4 scatter_custom_fusion
  16.6 6.9 %all-to-all-done = bf16[4,128,1024]{2,1,0:T(8,128)(2,1)S(1)} async-done(((bf16[4,128,1024]{2,1,0:T(8,128)(2,1)}), bf16[4,128,1024]{2,1,0:T(8,128)(2,1)S(1)}, u32[]{:S(2)}, u32[]{:S(2)}) %all-to-all-start) | async-done | bytes 1048608 | tf_op jit(solution)/shard_map/all_to_all | solution.py:12
  23.4 0.3 fusion
  23.7 0.3 convert_bitcast_fusion
  24.0 0.0 copy-start.5
  24.0 0.2 copy.49
  24.3 0.5 copy-done.5
  24.7 0.3 multiply_convert_fusion
  25.1 1.0 copy-done.2
  26.1 2.1 gather_fusion
  28.2 0.5 reshape_reshape_reshape.3
  28.7 0.6 copy.42
  29.3 10.5 %all_to_all.35 = bf16[64,2,1,1,3,1024]{5,0,4,3,2,1:T(8,128)(2,1)S(1)} all-to-all(bf16[64,2,1,1,3,1024]{5,0,4,3,2,1:T(8,128)(2,1)S(1)} %copy.42), channel_id=1, replica_groups=mesh['ep_0'=16,'ep_1'=4,'ep_2'=2,'tp'=4] {'ep_2'}, dimensions={1} | all-to-all | bytes 1572864 | tf_op jit(solution)/shard_map/all_to_all | solution.py:46
  39.7 0.8 copy.43
  40.5 59.1 %all_to_all.36 = bf16[64,2,1,1,3,1024]{5,1,4,3,2,0:T(2,128)(2,1)S(1)} all-to-all(bf16[64,2,1,1,3,1024]{5,1,4,3,2,0:T(2,128)(2,1)S(1)} %copy.43), channel_id=1, replica_groups=mesh['ep_0'=16,'ep_1'=4,'ep_2'=2,'tp'=4] {'ep_0','ep_1'}, dimensions={0} | all-to-all | bytes 1572864 | tf_op jit(solution)/shard_map/all_to_all | solution.py:46
  99.6 0.5 copy.44
  100.2 0.3 broadcast_in_dim.22
  100.5 2.1 broadcast_in_dim.23
  102.6 4.8 %all-to-all-start.3 = ((bf16[4,128,1,3,1024]{4,1,3,2,0:T(8,128)(2,1)}), bf16[4,128,1,3,1024]{4,1,3,2,0:T(8,128)(2,1)}, u32[]{:S(2)}, u32[]{:S(2)}) async-start(bf16[4,128,1,3,1024]{4,1,3,2,0:T(8,128)(2,1)} %broadcast_in_dim.23), calls=%async_computation.3 | async-start | bytes 6291456 | tf_op jit(solution)/shard_map/all_to_all | solution.py:12
  107.3 0.2 all-gather.2.cloned.1.call-start
  107.6 0.6 pad_maximum_fusion
  108.2 0.0 all-gather.2.cloned.1.call-update
  108.2 33.0 %all-to-all-done.3 = bf16[4,128,1,3,1024]{4,1,3,2,0:T(8,128)(2,1)} async-done(((bf16[4,128,1,3,1024]{4,1,3,2,0:T(8,128)(2,1)}), bf16[4,128,1,3,1024]{4,1,3,2,0:T(8,128)(2,1)}, u32[]{:S(2)}, u32[]{:S(2)}) %all-to-all-start.3) | async-done | bytes 3145760 | tf_op jit(solution)/shard_map/all_to_all | solution.py:12
  141.2 6.0 %copy.45 = bf16[128,1,3,4,1024]{4,3,0,2,1:T(4,128)(2,1)} copy(bf16[128,1,3,4,1024]{4,0,2,1,3:T(8,128)(2,1)} %bitcast.6) | data formatting | bytes 6291456 | tf_op jit(solution)/shard_map/transpose | solution.py:20
  147.2 6.2 %reshape.106 = bf16[128,3,4096]{2,0,1:T(8,128)(2,1)} reshape(bf16[128,1,3,4,1024]{4,3,0,2,1:T(4,128)(2,1)} %copy.45) | data formatting | bytes 6291456 | tf_op jit(solution)/shard_map/reshape.5
  153.4 3.0 %convolution_bitcast_fusion.1 = f32[128,1,3,128]{3,0,2,1:T(8,128)S(1)} fusion(bf16[128,3,4096]{2,0,1:T(8,128)(2,1)} %reshape.106, bf16[1,4096,128]{2,1,0:T(8,128)(2,1)S(1)} %copy-done.4), kind=kOutput, calls=%fused_computation.13 | convolution fusion | flops 402653184 | bytes 4390912 | tf_op jit(solution)/shard_map/secd,edh->sech/dot_general | solution.py:97
  156.5 0.1 copy-done.11
  156.6 1.0 fusion.5
  157.5 0.1 broadcast_in_dim.50
  157.6 8.6 %all_to_all.37 = bf16[4,128,1,3,128]{4,1,3,2,0:T(8,128)(2,1)S(1)} all-to-all(bf16[4,128,1,3,128]{4,1,3,2,0:T(8,128)(2,1)S(1)} %broadcast_in_dim.50), channel_id=1, replica_groups=mesh['ep_0'=16,'ep_1'=4,'ep_2'=2,'tp'=4] {'tp'}, dimensions={0} | all-to-all | bytes 786432 | tf_op jit(solution)/shard_map/all_to_all | solution.py:12
  166.2 0.3 copy.46
  166.5 0.2 reshape.109
  166.7 0.0 copy-done
  166.7 0.6 fusion.1
  167.3 0.0 copy-start.9
  167.3 0.0 copy-start.3
  167.3 1.6 copy.47
  169.0 15.1 %all-to-all-start.5 = ((bf16[128,1,3,1024]{3,2,1,0:T(4,128)(2,1)}), bf16[128,1,3,1024]{3,2,1,0:T(4,128)(2,1)S(1)}, u32[]{:S(2)}, u32[]{:S(2)}) async-start(bf16[128,1,3,1024]{3,2,1,0:T(4,128)(2,1)} %copy.47), calls=%async_computation.5 | async-start | bytes 2097152 | tf_op jit(solution)/shard_map/all_to_all | solution.py:106
  184.1 0.7 copy.35
  184.8 67.5 %all-gather.2.cloned.1.call-done = bf16[4096,256]{1,0:T(8,128)(2,1)} async-done(((bf16[32,256]{1,0:T(8,128)(2,1)}), bf16[4096,256]{1,0:T(8,128)(2,1)}) %all-gather.2.cloned.1.call-update) | async-done | bytes 2097168 | tf_op jit(solution)/shard_map/all_gather | solution.py:30
  252.3 1.8 fusion.8
  254.1 0.1 copy-done.10
  254.2 0.4 fusion.6
  254.7 0.1 copy.48
  254.8 0.0 all-to-all-done.5
  254.8 0.7 broadcast_in_dim.51
  255.5 3.6 %all-to-all-start.6 = ((bf16[4,128,128]{1,2,0:T(8,128)(2,1)}), bf16[4,128,128]{1,2,0:T(8,128)(2,1)S(1)}, u32[]{:S(2)}, u32[]{:S(2)}) async-start(bf16[4,128,128]{1,2,0:T(8,128)(2,1)} %broadcast_in_dim.51), calls=%async_computation.6 | async-start | bytes 262144 | tf_op jit(solution)/shard_map/all_to_all | solution.py:12
  259.0 0.7 reshape.111
  259.7 1.2 gather_fusion.1
  260.9 0.7 reshape.114
  261.6 2.2 multiply_reduce_fusion
  263.8 0.1 all-to-all-done.6
  263.9 2.3 fusion.2
  (31 shorter events, 0.2 us)
Async XLA Ops:
  6.5 160.2 %copy-start = (bf16[1,512,1024]{2,1,0:T(8,128)(2,1)S(1)}, bf16[1,512,1024]{2,1,0:T(8,128)(2,1)}, u32[]{:S(2)}) copy-start(bf16[1,512,1024]{2,1,0:T(8,128)(2,1)} %param.16) | copy-start | bytes 3145732
  6.5 7.2 %copy-start.8 = (s32[128,2]{0,1:T(2,128)S(1)}, s32[128,2]{0,1:T(2,128)}, u32[]{:S(2)}) copy-start(s32[128,2]{0,1:T(2,128)} %param.12) | copy-start | bytes 3076
  8.7 14.8 %all-to-all-start = ((bf16[4,128,1024]{2,1,0:T(8,128)(2,1)}), bf16[4,128,1024]{2,1,0:T(8,128)(2,1)S(1)}, u32[]{:S(2)}, u32[]{:S(2)}) async-start(bf16[4,128,1024]{2,1,0:T(8,128)(2,1)} %broadcast_in_dim.18), calls=%async_computation | async-start | bytes 2097152 | tf_op jit(solution)/shard_map/all_to_all | solution.py:12
  24.0 0.7 copy-start.5
  25.0 1.1 copy-start.2
  102.5 5.0 %copy-start.6 = (bf16[32,128]{1,0:T(8,128)(2,1)S(1)}, bf16[32,128]{1,0:T(8,128)(2,1)}, u32[]{:S(2)}) copy-start(bf16[32,128]{1,0:T(8,128)(2,1)} %param.18) | copy-start | bytes 24580
  102.6 5.0 %copy-start.7 = (bf16[32,128]{1,0:T(8,128)(2,1)S(1)}, bf16[32,128]{1,0:T(8,128)(2,1)}, u32[]{:S(2)}) copy-start(bf16[32,128]{1,0:T(8,128)(2,1)} %param.17) | copy-start | bytes 24580
  102.6 38.7 %all-to-all-start.3 = ((bf16[4,128,1,3,1024]{4,1,3,2,0:T(8,128)(2,1)}), bf16[4,128,1,3,1024]{4,1,3,2,0:T(8,128)(2,1)}, u32[]{:S(2)}, u32[]{:S(2)}) async-start(bf16[4,128,1,3,1024]{4,1,3,2,0:T(8,128)(2,1)} %broadcast_in_dim.23), calls=%async_computation.3 | async-start | bytes 6291456 | tf_op jit(solution)/shard_map/all_to_all | solution.py:12
  107.3 145.0 %all-gather.2.cloned.1.call-start = ((), (), s32[]{:S(2)}) async-start(), calls=%async_computation.7 | async-start | bytes 2113536 | tf_op jit(solution)/shard_map/all_gather | solution.py:30
  147.2 6.2 %copy-start.4 = (bf16[1,4096,128]{2,1,0:T(8,128)(2,1)S(1)}, bf16[1,4096,128]{2,1,0:T(8,128)(2,1)}, u32[]{:S(2)}) copy-start(bf16[1,4096,128]{2,1,0:T(8,128)(2,1)} %param.14) | copy-start | bytes 3145732
  153.4 3.0 %copy-start.1 = (bf16[128,3,4096]{2,0,1:T(8,128)(2,1)S(1)}, bf16[128,3,4096]{2,0,1:T(8,128)(2,1)}, u32[]{:S(2)}) copy-start(bf16[128,3,4096]{2,0,1:T(8,128)(2,1)} %reshape.106) | copy-start | bytes 9437188
  153.4 3.1 %copy-start.11 = (bf16[1,4096,128]{2,1,0:T(8,128)(2,1)S(1)}, bf16[1,4096,128]{2,1,0:T(8,128)(2,1)}, u32[]{:S(2)}) copy-start(bf16[1,4096,128]{2,1,0:T(8,128)(2,1)} %param.15) | copy-start | bytes 3145732
  167.3 16.8 %copy-start.9 = (f32[128,2]{0,1:T(2,128)S(1)}, f32[128,2]{0,1:T(2,128)}, u32[]{:S(2)}) copy-start(f32[128,2]{0,1:T(2,128)} %param.13) | copy-start | bytes 3076
  167.3 85.0 %copy-start.3 = (bf16[128,4096]{1,0:T(8,128)(2,1)S(1)}, bf16[128,4096]{1,0:T(8,128)(2,1)}, u32[]{:S(2)}) copy-start(bf16[128,4096]{1,0:T(8,128)(2,1)} %copy-done.2) | copy-start | bytes 3145732
  169.0 85.8 %all-to-all-start.5 = ((bf16[128,1,3,1024]{3,2,1,0:T(4,128)(2,1)}), bf16[128,1,3,1024]{3,2,1,0:T(4,128)(2,1)S(1)}, u32[]{:S(2)}, u32[]{:S(2)}) async-start(bf16[128,1,3,1024]{3,2,1,0:T(4,128)(2,1)} %copy.47), calls=%async_computation.5 | async-start | bytes 2097152 | tf_op jit(solution)/shard_map/all_to_all | solution.py:106
  252.3 1.9 copy-start.10
  255.5 8.4 %all-to-all-start.6 = ((bf16[4,128,128]{1,2,0:T(8,128)(2,1)}), bf16[4,128,128]{1,2,0:T(8,128)(2,1)S(1)}, u32[]{:S(2)}, u32[]{:S(2)}) async-start(bf16[4,128,128]{1,2,0:T(8,128)(2,1)} %broadcast_in_dim.51), calls=%async_computation.6 | async-start | bytes 262144 | tf_op jit(solution)/shard_map/all_to_all | solution.py:12
Sparse Core Ops, SparseCore 0:
  111.3 140.9 all-gather.1
where the time goes:
time: 274 us; the launch traced here: 273 us
  waiting for transfers between devices  107 us (39%)
  blocking collectives  78.2 us (29%)
  local copies, waits for them, and re-layouts  31.8 us (12%)
  starting transfers between devices  28.6 us (10%)
  between operations  13.7 us (5%)
  matrix products  9.04 us (3%)
  other arithmetic  4.13 us (2%)
    all_to_all x2, blocking collectives, turned_blocks(): filled = lax.all_to_all(filled, axes[k], k, k, tiled=True)  69.5 us
    all_gather x1, waiting for transfers between devices, sent_together(): filled, at, outs = (lax.all_gather(both, axis, axis=dim, tiled=True), 0, [])  67.5 us
    all_to_all x3, waiting for transfers between devices, copy_for_each(): lax.all_to_all(jnp.broadcast_to(value[None], (peers, *value.shape)), axis...  39.9 us
    all_to_all x1, starting transfers between devices, shards(): lax.all_to_all(expert_out, EP, split_axis=0, concat_axis=0, tiled=True)  15.1 us
    all_to_all x3, starting transfers between devices, copy_for_each(): lax.all_to_all(jnp.broadcast_to(value[None], (peers, *value.shape)), axis...  13.3 us
    all_to_all x1, blocking collectives, copy_for_each(): lax.all_to_all(jnp.broadcast_to(value[None], (peers, *value.shape)), axis...  8.62 us
    another operation x5, local copies, waits for them, and re-layouts  6.38 us
    transpose x2, local copies, waits for them, and re-layouts, laid_out(): return jnp.moveaxis(blocks, 0, dim).reshape(shape)  6.31 us
  transfers between devices with their start and end apart: 5, of which 4 were waited for; matrix products, arithmetic and copies ran while one was open for 11% of the time, Pallas kernels for 0%

commit v1 on v0

--- a/solution.py
+++ b/solution.py
@@ -1,6 +1,8 @@
 import jax
 import jax.numpy as jnp
 from jax import lax
+from jax.experimental import pallas as pl
+from jax.experimental.pallas import tpu as pltpu
 from jax.sharding import Mesh
 from jax.sharding import PartitionSpec as P
 
@@ -53,6 +55,61 @@
     return laid_out(turned_blocks(blocks, groups, sequence), concat_dim)
 
 
+MESH = pl.DeviceIdType.MESH
+
+
+def exchange_kernel(src, dst, send_sem, recv_sem):
+    z, x, c, y = (lax.axis_index(a) for a in ("ep_0", "ep_1", "ep_2", "tp"))
+    me = (z * 4 + x) * 2 + c
+
+    def peer(i):
+        step = i // 8
+        half = (step + 1) // 2
+        dz = (8 - half) * (step % 2) + (8 + half) * (1 - step % 2)
+        w = i % 8
+        return (z + dz) % 16, (x + w // 2) % 4, (c + w % 2) % 2, y
+
+    barrier = pltpu.get_barrier_semaphore()
+
+    def greet(i, _):
+        pl.semaphore_signal(barrier, inc=1, device_id=peer(i), device_id_type=MESH)
+        return 0
+
+    lax.fori_loop(0, 120, greet, 0)
+    lax.fori_loop(121, 128, greet, 0)
+    pl.semaphore_wait(barrier, 127)
+
+    def send(i, _):
+        p = peer(i)
+        pltpu.make_async_remote_copy(
+            src_ref=src.at[(p[0] * 4 + p[1]) * 2 + p[2]],
+            dst_ref=dst.at[me],
+            send_sem=send_sem,
+            recv_sem=recv_sem,
+            device_id=p,
+            device_id_type=MESH,
+        ).start()
+        return 0
+
+    lax.fori_loop(0, 120, send, 0)
+    lax.fori_loop(121, 128, send, 0)
+    dst[me] = src[me]
+    most = pl.ds(0, 127)
+    pltpu.make_async_copy(src.at[most], dst.at[most], recv_sem).wait()
+    pltpu.make_async_copy(src.at[most], src.at[most], send_sem).wait()
+
+
+def exchange(blocks):
+    return pl.pallas_call(
+        exchange_kernel,
+        out_shape=jax.ShapeDtypeStruct(blocks.shape, blocks.dtype),
+        in_specs=[pl.BlockSpec(memory_space=pltpu.VMEM)],
+        out_specs=pl.BlockSpec(memory_space=pltpu.VMEM),
+        scratch_shapes=[pltpu.SemaphoreType.DMA, pltpu.SemaphoreType.DMA],
+        compiler_params=pltpu.CompilerParams(collective_id=0, has_side_effects=True),
+    )(blocks)
+
+
 def shards(
     tokens,
     norm_gain,
@@ -91,8 +148,8 @@
     owner = jnp.full((n_exp * cap,), tok_rows, jnp.int32).at[dest].set(local_tok)
     own_part = lax.dynamic_slice_in_dim(normed, lax.axis_index("tp") * quarter, quarter, 1)
     padded = jnp.concatenate([own_part, jnp.zeros((1, quarter), jnp.bfloat16)], axis=0)
-    outgoing = padded[owner].reshape(n_ep, exp_dev, cap, quarter)
-    arrived = core_and_chips(outgoing, (("ep_0", "ep_1"), "ep_2"), (1, 0), 0, 0)
+    outgoing = padded[owner].reshape(n_ep, 2, exp_dev * cap * quarter // 2)
+    arrived = exchange(outgoing).reshape(n_ep, exp_dev, cap, quarter)
     received = collect(arrived, "tp", 3)
     gate_vals = jnp.einsum(
         "secd,edh->sech", received, gate_proj, preferred_element_type=jnp.float32
@@ -103,7 +160,7 @@
     expert_out = jnp.einsum(
         "sech,ehd->secd", collect(expert_hidden, "tp", 3), rows, preferred_element_type=jnp.float32
     ).astype(jnp.bfloat16)
-    returned = lax.all_to_all(expert_out, EP, split_axis=0, concat_axis=0, tiled=True)
+    returned = exchange(expert_out.reshape(n_ep, 2, -1))
     picked = returned.reshape(n_exp * cap, quarter)[dest].reshape(tok_rows, top, quarter)
     routed = jnp.sum(expert_gates[:, :, None] * picked.astype(jnp.float32), axis=1)
     return (routed + shared_out).astype(jnp.bfloat16)

time: 274 us -> 241 us (0.88)
  Pallas kernels: 0 us -> 112 us
  waiting for transfers between devices: 107 us -> 16.6 us
  blocking collectives: 78.2 us -> 39.7 us
  starting transfers between devices: 28.6 us -> 12 us
    pallas_call x0 -> x2, Pallas kernels: none -> 112 us  [exchange(): pl.pallas_call(exchange_kernel, out_shape=jax.ShapeDtypeStruct(blocks.sha...]
    all_to_all x2 -> x0, blocking collectives: 69.5 us -> none  [turned_blocks(): filled = lax.all_to_all(filled, axes[k], k, k, tiled=True)]
    all_gather x1, waiting for transfers between devices: 67.5 us -> 0.02 us  [sent_together(): filled, at, outs = (lax.all_gather(both, axis, axis=dim, tiled=True), 0, [])]
    all_to_all x1, blocking collectives: 8.62 us -> 39.7 us  [copy_for_each(): lax.all_to_all(jnp.broadcast_to(value[None], (peers, *value.shape)), axis...]
    all_to_all x3, waiting for transfers between devices: 39.9 us -> 16.5 us  [copy_for_each(): lax.all_to_all(jnp.broadcast_to(value[None], (peers, *value.shape)), axis...]
    all_to_all x1 -> x0, starting transfers between devices: 15.1 us -> none  [shards(): lax.all_to_all(expert_out, EP, split_axis=0, concat_axis=0, tiled=True)]
    reshape x0 -> x2, local copies, waits for them, and re-layouts: none -> 3.23 us  [the longest x1 1.85 us: shards(): returned = exchange(expert_out.reshape(n_ep, 2, -1))]
    another operation x7 -> x5, local copies, waits for them, and re-layouts: 7.46 us -> 6.37 us
  transfers between devices with their start and end apart: 5 -> 4, of which waited for: 4 -> 3; matrix products, arithmetic and copies ran while one was open for 11% -> 15% of each run, Pallas kernels for 0% -> 47%
where the time goes in v1:
time: 241 us; the launch traced here: 240 us
  Pallas kernels  112 us (46%)
  blocking collectives  39.7 us (16%)
  local copies, waits for them, and re-layouts  31.7 us (13%)
  waiting for transfers between devices  16.6 us (7%)
  between operations  13.7 us (6%)
  starting transfers between devices  12 us (5%)
  matrix products  10.5 us (4%)
  other arithmetic  4.07 us (2%)
    pallas_call x2, Pallas kernels, exchange(): pl.pallas_call(exchange_kernel, out_shape=jax.ShapeDtypeStruct(blocks.sha...  112 us
    all_to_all x1, blocking collectives, copy_for_each(): lax.all_to_all(jnp.broadcast_to(value[None], (peers, *value.shape)), axis...  39.7 us
    all_to_all x3, waiting for transfers between devices, copy_for_each(): lax.all_to_all(jnp.broadcast_to(value[None], (peers, *value.shape)), axis...  16.5 us
    all_to_all x3, starting transfers between devices, copy_for_each(): lax.all_to_all(jnp.broadcast_to(value[None], (peers, *value.shape)), axis...  12 us
    another operation x5, local copies, waits for them, and re-layouts  6.37 us
  transfers between devices with their start and end apart: 4, of which 3 were waited for; matrix products, arithmetic and copies ran while one was open for 15% of the time, Pallas kernels for 47%

profile of v1, /device:TPU:1, one launch (start us, length us, event | category | flops | bytes accessed | tf_op | source)
XLA Modules:
  0.0 240.0 jit_solution(3001807904256825626)
XLA Ops:
  6.5 0.0 copy-start
  6.5 0.0 all-gather.2.cloned.1.call-start
  6.5 1.4 pad_maximum_fusion
  8.0 0.0 all-gather.2.cloned.1.call-update
  8.0 2.1 broadcast_in_dim.18
  10.0 5.0 %all-to-all-start = ((bf16[4,128,1024]{2,1,0:T(8,128)(2,1)}), bf16[4,128,1024]{2,1,0:T(8,128)(2,1)S(1)}, u32[]{:S(2)}, u32[]{:S(2)}) async-start(bf16[4,128,1024]{2,1,0:T(8,128)(2,1)} %broadcast_in_dim.18), calls=%async_computation | async-start | bytes 2097152 | tf_op jit(solution)/shard_map/all_to_all | solution.py:14
  15.0 0.0 copy-done.6
  15.0 0.1 copy.28
  15.2 0.1 eq.29
  15.3 0.1 copy.30
  15.4 0.2 fusion.13
  15.7 0.1 eq.25
  15.9 0.1 copy.27
  16.0 0.1 mul.74
  16.2 0.1 reshape.143
  16.3 0.2 fusion.15
  16.5 1.4 scatter_custom_fusion
  17.9 6.9 %all-to-all-done = bf16[4,128,1024]{2,1,0:T(8,128)(2,1)S(1)} async-done(((bf16[4,128,1024]{2,1,0:T(8,128)(2,1)}), bf16[4,128,1024]{2,1,0:T(8,128)(2,1)S(1)}, u32[]{:S(2)}, u32[]{:S(2)}) %all-to-all-start) | async-done | bytes 1048608 | tf_op jit(solution)/shard_map/all_to_all | solution.py:14
  24.8 0.3 fusion
  25.1 0.3 convert_bitcast_fusion
  25.4 0.0 copy-start.5
  25.4 0.2 copy.39
  25.6 0.5 copy-done.5
  26.1 0.3 multiply_convert_fusion
  26.4 0.0 copy-start.2
  26.4 1.0 copy-done.2
  27.4 2.1 gather_fusion
  29.5 1.4 reshape.112.src
  30.9 61.9 %shard_map.100 = bf16[128,2,1536]{2,1,0:T(2,128)(2,1)} custom-call(bf16[128,2,1536]{2,1,0:T(2,128)(2,1)} %reshape.112.src), custom_call_target="tpu_custom_call" | custom-call | tf_op jit(solution)/shard_map/pallas_call | solution.py:103
  92.8 2.3 copy.32
  95.2 0.3 copy.33
  95.4 0.4 broadcast_in_dim.23
  95.8 39.7 %all_to_all.20 = bf16[4,128,1,3,1024]{4,1,3,2,0:T(8,128)(2,1)S(1)} all-to-all(bf16[4,128,1,3,1024]{4,1,3,2,0:T(8,128)(2,1)S(1)} %broadcast_in_dim.23), channel_id=1, replica_groups=mesh['ep_0'=16,'ep_1'=4,'ep_2'=2,'tp'=4] {'tp'}, dimensions={0} | all-to-all | bytes 6291456 | tf_op jit(solution)/shard_map/all_to_all | solution.py:14
  135.5 4.1 %copy.34 = bf16[128,1,3,4,1024]{4,3,0,2,1:T(4,128)(2,1)} copy(bf16[128,1,3,4,1024]{4,0,2,1,3:T(8,128)(2,1)S(1)} %bitcast.76) | data formatting | bytes 6291456 | tf_op jit(solution)/shard_map/transpose | solution.py:22
  139.6 6.2 %reshape.113 = bf16[128,3,4096]{2,0,1:T(8,128)(2,1)} reshape(bf16[128,1,3,4,1024]{4,3,0,2,1:T(4,128)(2,1)} %copy.34) | data formatting | bytes 6291456 | tf_op jit(solution)/shard_map/reshape.5
  145.8 0.0 copy-done.4
  145.8 3.0 %convolution_bitcast_fusion.1 = f32[128,1,3,128]{3,0,2,1:T(8,128)S(1)} fusion(bf16[128,3,4096]{2,0,1:T(8,128)(2,1)} %reshape.113, bf16[1,4096,128]{2,1,0:T(8,128)(2,1)S(1)} %copy-done.4), kind=kOutput, calls=%fused_computation.13 | convolution fusion | flops 402653184 | bytes 4390912 | tf_op jit(solution)/shard_map/secd,edh->sech/dot_general | solution.py:154
  148.9 0.0 copy-done.1
  148.9 0.1 copy-done.8
  149.0 1.0 fusion.5
  149.9 0.8 broadcast_in_dim.50
  150.8 3.6 %all-to-all-start.2 = ((bf16[4,128,1,3,128]{4,1,3,2,0:T(8,128)(2,1)}), bf16[4,128,1,3,128]{4,1,3,2,0:T(8,128)(2,1)S(1)}, u32[]{:S(2)}, u32[]{:S(2)}) async-start(bf16[4,128,1,3,128]{4,1,3,2,0:T(8,128)(2,1)} %broadcast_in_dim.50), calls=%async_computation.2 | async-start | bytes 786432 | tf_op jit(solution)/shard_map/all_to_all | solution.py:14
  154.4 0.0 copy-done.7
  154.4 0.1 copy.25
  154.5 6.2 %all-to-all-done.2 = bf16[4,128,1,3,128]{4,1,3,2,0:T(8,128)(2,1)S(1)} async-done(((bf16[4,128,1,3,128]{4,1,3,2,0:T(8,128)(2,1)}), bf16[4,128,1,3,128]{4,1,3,2,0:T(8,128)(2,1)S(1)}, u32[]{:S(2)}, u32[]{:S(2)}) %all-to-all-start.2) | async-done | bytes 393248 | tf_op jit(solution)/shard_map/all_to_all | solution.py:14
  160.7 0.3 copy.35
  161.0 0.2 reshape.116
  161.2 0.0 copy-done
  161.2 0.6 fusion.1
  161.8 0.4 copy.36
  162.2 1.8 copy.37.src
  164.0 49.8 %shard_map.101 = bf16[128,2,1536]{2,1,0:T(2,128)(2,1)} custom-call(bf16[128,2,1536]{2,1,0:T(2,128)(2,1)} %copy.37.src), custom_call_target="tpu_custom_call" | custom-call | tf_op jit(solution)/shard_map/pallas_call | solution.py:103
  213.9 2.5 %reshape.119 = bf16[384,1024]{1,0:T(8,128)(2,1)S(1)} reshape(bf16[128,2,1536]{2,1,0:T(2,128)(2,1)} %shard_map.101) | data formatting | bytes 1572864 | tf_op jit(solution)/shard_map/reshape | solution.py:164
  216.3 1.2 gather_fusion.1
  217.5 0.7 reshape.122
  218.2 0.0 all-gather.2.cloned.1.call-done
  218.2 2.0 fusion.8
  220.3 1.6 fusion.6
  221.9 0.1 copy.38
  222.0 0.7 broadcast_in_dim.51
  222.7 3.3 %all-to-all-start.3 = ((bf16[4,128,128]{1,2,0:T(8,128)(2,1)}), bf16[4,128,128]{1,2,0:T(8,128)(2,1)S(1)}, u32[]{:S(2)}, u32[]{:S(2)}) async-start(bf16[4,128,128]{1,2,0:T(8,128)(2,1)} %broadcast_in_dim.51), calls=%async_computation.3 | async-start | bytes 262144 | tf_op jit(solution)/shard_map/all_to_all | solution.py:14
  226.0 1.3 multiply_reduce_fusion
  227.4 3.4 %all-to-all-done.3 = bf16[4,128,128]{1,2,0:T(8,128)(2,1)S(1)} async-done(((bf16[4,128,128]{1,2,0:T(8,128)(2,1)}), bf16[4,128,128]{1,2,0:T(8,128)(2,1)S(1)}, u32[]{:S(2)}, u32[]{:S(2)}) %all-to-all-start.3) | async-done | bytes 131104 | tf_op jit(solution)/shard_map/all_to_all | solution.py:14
  230.9 2.3 fusion.2
  (22 shorter events, 0.2 us)
Async XLA Ops:
  6.5 154.7 %copy-start = (bf16[1,512,1024]{2,1,0:T(8,128)(2,1)S(1)}, bf16[1,512,1024]{2,1,0:T(8,128)(2,1)}, u32[]{:S(2)}) copy-start(bf16[1,512,1024]{2,1,0:T(8,128)(2,1)} %param.16) | copy-start | bytes 3145732
  6.5 8.5 %copy-start.6 = (s32[128,2]{0,1:T(2,128)S(1)}, s32[128,2]{0,1:T(2,128)}, u32[]{:S(2)}) copy-start(s32[128,2]{0,1:T(2,128)} %param.12) | copy-start | bytes 3076
  6.5 211.7 %all-gather.2.cloned.1.call-start = ((), (), s32[]{:S(2)}) async-start(), calls=%async_computation.4 | async-start | bytes 2113536 | tf_op jit(solution)/shard_map/all_gather | solution.py:32
  10.0 14.8 %all-to-all-start = ((bf16[4,128,1024]{2,1,0:T(8,128)(2,1)}), bf16[4,128,1024]{2,1,0:T(8,128)(2,1)S(1)}, u32[]{:S(2)}, u32[]{:S(2)}) async-start(bf16[4,128,1024]{2,1,0:T(8,128)(2,1)} %broadcast_in_dim.18), calls=%async_computation | async-start | bytes 2097152 | tf_op jit(solution)/shard_map/all_to_all | solution.py:14
  25.4 0.7 copy-start.5
  26.4 1.0 copy-start.2
  139.6 6.2 %copy-start.4 = (bf16[1,4096,128]{2,1,0:T(8,128)(2,1)S(1)}, bf16[1,4096,128]{2,1,0:T(8,128)(2,1)}, u32[]{:S(2)}) copy-start(bf16[1,4096,128]{2,1,0:T(8,128)(2,1)} %param.14) | copy-start | bytes 3145732
  145.8 3.0 %copy-start.1 = (bf16[128,3,4096]{2,0,1:T(8,128)(2,1)S(1)}, bf16[128,3,4096]{2,0,1:T(8,128)(2,1)}, u32[]{:S(2)}) copy-start(bf16[128,3,4096]{2,0,1:T(8,128)(2,1)} %reshape.113) | copy-start | bytes 9437188
  145.8 3.1 %copy-start.8 = (bf16[1,4096,128]{2,1,0:T(8,128)(2,1)S(1)}, bf16[1,4096,128]{2,1,0:T(8,128)(2,1)}, u32[]{:S(2)}) copy-start(bf16[1,4096,128]{2,1,0:T(8,128)(2,1)} %param.15) | copy-start | bytes 3145732
  149.0 5.4 %copy-start.7 = (f32[128,2]{0,1:T(2,128)S(1)}, f32[128,2]{0,1:T(2,128)}, u32[]{:S(2)}) copy-start(f32[128,2]{0,1:T(2,128)} %param.13) | copy-start | bytes 3076
  150.8 10.0 %all-to-all-start.2 = ((bf16[4,128,1,3,128]{4,1,3,2,0:T(8,128)(2,1)}), bf16[4,128,1,3,128]{4,1,3,2,0:T(8,128)(2,1)S(1)}, u32[]{:S(2)}, u32[]{:S(2)}) async-start(bf16[4,128,1,3,128]{4,1,3,2,0:T(8,128)(2,1)} %broadcast_in_dim.50), calls=%async_computation.2 | async-start | bytes 786432 | tf_op jit(solution)/shard_map/all_to_all | solution.py:14
  218.2 2.1 copy-start.3
  222.7 8.1 %all-to-all-start.3 = ((bf16[4,128,128]{1,2,0:T(8,128)(2,1)}), bf16[4,128,128]{1,2,0:T(8,128)(2,1)S(1)}, u32[]{:S(2)}, u32[]{:S(2)}) async-start(bf16[4,128,128]{1,2,0:T(8,128)(2,1)} %broadcast_in_dim.51), calls=%async_computation.3 | async-start | bytes 262144 | tf_op jit(solution)/shard_map/all_to_all | solution.py:14
Sparse Core Ops, SparseCore 0:
  10.5 155.6 all-gather.1

commit v2 on v0

v2 whole, which is shorter than its diff:
```python
import jax
import jax.numpy as jnp
from jax import lax
from jax.experimental import pallas as pl
from jax.experimental.pallas import tpu as pltpu
from jax.sharding import Mesh
from jax.sharding import PartitionSpec as P

EP = ("ep_0", "ep_1", "ep_2")
MESH = pl.DeviceIdType.MESH
BF16 = jnp.bfloat16
F32 = jnp.float32
PLANES, PER_PLANE, PEERS = 16, 8, 128
BATCHES = 4


def offset_of(i):
    half = (i + 1) // 2
    return (i % 2) * half + (1 - i % 2) * ((PLANES - half) % PLANES)


def dot(a, b):
    return jnp.dot(a, b, preferred_element_type=F32)


def parity(shape, axis):
    return lax.broadcasted_iota(jnp.int32, shape, axis) % 2


def swap_pairs(v):
    n = v.shape[0]
    return jnp.where(
        parity(v.shape, 0) == 0, pltpu.roll(v, n - 1, 0), pltpu.roll(v, 1, 0)
    )


def silu_mul(g, u):
    return g / (1.0 + jnp.exp(-g)) * u


def layer_kernel(
    tokens,
    gain,
    ids,
    ids_t,
    gates,
    gate_hbm,
    up_hbm,
    down_hbm,
    shared_gate,
    shared_up,
    shared_down_hbm,
    out,
    send,
    rows,
    mixed_in,
    hidden,
    give,
    got,
    all_tokens,
    shared_w,
    shared_hidden,
    gate_up,
    down,
    shared_down,
    load_sem,
    send_sem,
    row_sem,
    fwd_send,
    fwd_sem,
    hid_send,
    hid_sem,
    give_send,
    got_sem,
    tok_send,
    tok_sem,
    ring_send,
    ring_sem,
    wx_send,
    wx_sem,
    wc_send,
    wc_sem,
    sh_send,
    sh_sem,
):
    z, x, c, y = (lax.axis_index(a) for a in (*EP, "tp"))
    w = x * 2 + c
    me = z * PER_PLANE + w
    tps = (1, 3, 2)

    def remote(src, dst, ssem, rsem, device):
        return pltpu.make_async_remote_copy(
            src_ref=src,
            dst_ref=dst,
            send_sem=ssem,
            recv_sem=rsem,
            device_id=device,
            device_id_type=MESH,
        )

    def drain(ref, sem):
        pltpu.make_async_copy(ref, ref, sem).wait()

    def ep_peer(dz, k):
        return (z + dz) % PLANES, (x + k // 2) % 4, (c + k % 2) % 2, y

    def tp_peer(d):
        return z, x, c, (y + d) % 4

    def index_of(device):
        return (device[0] * 4 + device[1]) * 2 + device[2]

    barrier = pltpu.get_barrier_semaphore()

    def greet(f, _):
        peer = ep_peer(offset_of(f // PER_PLANE), f % PER_PLANE)
        pl.semaphore_signal(barrier, inc=1, device_id=peer, device_id_type=MESH)
        return 0

    lax.fori_loop(1, PEERS, greet, 0)
    for d in tps:
        pl.semaphore_signal(barrier, inc=1, device_id=tp_peer(d), device_id_type=MESH)

    loads = [
        pltpu.make_async_copy(gate_hbm.at[0], gate_up.at[:, pl.ds(0, 128)], load_sem.at[0]),
        pltpu.make_async_copy(up_hbm.at[0], gate_up.at[:, pl.ds(128, 128)], load_sem.at[1]),
        pltpu.make_async_copy(down_hbm.at[0], down, load_sem.at[2]),
        pltpu.make_async_copy(shared_down_hbm, shared_down, load_sem.at[3]),
    ]
    for load in loads:
        load.start()

    tok = tokens[...]
    expert = lax.broadcasted_iota(jnp.int32, (128, 128), 0)
    lane = lax.broadcasted_iota(jnp.int32, (128, 128), 1)
    first_t, second_t = ids_t[0:1, :], ids_t[1:2, :]
    names0, names1 = (expert == first_t).astype(F32), (expert == second_t).astype(F32)
    before = dot((names0 + names1).astype(BF16), (expert < lane).astype(BF16))
    slot0 = jnp.sum(names0 * before, axis=0, keepdims=True).astype(jnp.int32)
    slot1 = jnp.sum(names1 * before, axis=0, keepdims=True).astype(jnp.int32)

    row = lax.broadcasted_iota(jnp.int32, (256, 128), 0)
    pair0 = jnp.where(slot0 < 2, 2 * first_t + slot0, -1)
    pair1 = jnp.where(slot1 < 2, 2 * second_t + slot1, -1)
    last0 = jnp.where(slot0 == 2, first_t, -1)
    last1 = jnp.where(slot1 == 2, second_t, -1)
    pick_pair = ((row == pair0) | (row == pair1)).astype(BF16)
    pick_last = ((row // 2 == last0) | (row // 2 == last1)).astype(BF16)
    send[:, :, :1024] = dot(pick_pair, tok).astype(BF16).reshape(128, 2, 1024)
    whole = dot(pick_last, tok)
    halves = jnp.where(parity((256, 512), 0) == 0, whole[:, :512], whole[:, 512:])
    send[:, :, 1024:] = halves.astype(BF16).reshape(128, 2, 512)
    rows[y, me] = send[me]
    all_tokens[y] = tok
    shared_w[z, w, :, :128] = shared_gate[...]
    shared_w[z, w, :, 128:] = shared_up[...]

    pl.semaphore_wait(barrier, PEERS - 1 + 3)

    def dispatch(f, _):
        i = f // PER_PLANE
        peer = ep_peer(offset_of(i), f % PER_PLANE)
        remote(send.at[index_of(peer)], rows.at[y, me], send_sem, row_sem.at[i], peer).start()
        return 0

    lax.fori_loop(1, PEERS, dispatch, 0)

    def ring(h, side):
        plane = (z + PLANES - (h - 1)) % PLANES if side == 0 else (z + h - 1) % PLANES
        block = shared_w.at[plane, w]
        peer = ep_peer(1 if side == 0 else PLANES - 1, 0)
        return remote(block, block, ring_send, ring_sem.at[side, h - 1], peer)

    def ring_step(h):
        for side in (0, 1):
            if 1 < h and not (side == 1 and h - 1 > 7):
                ring(h - 1, side).wait_recv()
            if h <= (8, 7)[side]:
                ring(h, side).start()

    ring_step(1)

    def plane_of(i):
        return (z + PLANES - offset_of(i)) % PLANES

    def forward(i):
        group = rows.at[y, pl.ds(plane_of(i) * PER_PLANE, PER_PLANE)]
        if i == 0:
            drain(rows.at[y, pl.ds(0, PER_PLANE - 1)], row_sem.at[0])
        else:
            drain(group, row_sem.at[i])
        for n, d in enumerate(tps):
            remote(group, group, fwd_send, fwd_sem.at[n, i], tp_peer(d)).start()

    even = parity((64, 512), 0) == 0

    def expert_in(b):
        for i in range(4 * b, 4 * b + 4):
            for n in range(3):
                drain(rows.at[0, pl.ds(0, PER_PLANE)], fwd_sem.at[n, i])

        def batch(t):
            parts = [
                rows[t, pl.ds(plane_of(i) * PER_PLANE, PER_PLANE)].reshape(16, 1536)
                for i in range(4 * b, 4 * b + 4)
            ]
            return jnp.concatenate(parts, axis=0)

        square_pair, square_last = jnp.zeros((64, 1), F32), jnp.zeros((64, 1), F32)
        for t in range(4):
            v = batch(t).astype(F32)
            sq = v * v
            square_pair += jnp.sum(sq[:, :1024], axis=1, keepdims=True)
            square_last += jnp.sum(sq[:, 1024:], axis=1, keepdims=True)
        last_wide = jnp.broadcast_to(square_last, (64, 128))
        square_last = (last_wide + swap_pairs(last_wide))[:, :1]
        scale_pair = lax.rsqrt(square_pair / 4096.0 + 1e-06)
        scale_last = lax.rsqrt(square_last / 4096.0 + 1e-06)
        for t in range(4):
            v = batch(t).astype(F32)
            g = gain[t : t + 1, :]
            mixed_in[0:64, t * 1024 : (t + 1) * 1024] = (v[:, :1024] * scale_pair * g).astype(BF16)
            last = v[:, 1024:] * scale_last
            for p in (0, 1):
                mine = even if p == 0 else jnp.logical_not(even)
                part = jnp.where(mine, last * g[:, p * 512 : (p + 1) * 512], 0.0)
                at = t * 1024 + p * 512
                mixed_in[64:128, at : at + 512] = part.astype(BF16)
        both = dot(mixed_in[...], gate_up[...])
        tail = both[64:]
        both = jnp.concatenate([both[:64], tail + swap_pairs(tail)], axis=0)
        hidden[y, b] = silu_mul(both[:, :128], both[:, 128:]).astype(BF16)
        for n, d in enumerate(tps):
            remote(hidden.at[y, b], hidden.at[y, b], hid_send, hid_sem.at[n, b], tp_peer(d)).start()

    def expert_out(b):
        for n in range(3):
            drain(hidden.at[0, 0], hid_sem.at[n, b])
        full = jnp.concatenate([hidden[t, b] for t in range(4)], axis=1)
        res = dot(full, down[...])
        tail = jnp.where(even, res[64:, :512], res[64:, 512:])
        res = jnp.concatenate([res[:64], tail], axis=1).astype(BF16)
        for j in range(4):
            i = 4 * b + j
            plane = plane_of(i)
            give[pl.ds(plane * PER_PLANE, PER_PLANE)] = res[16 * j : 16 * j + 16].reshape(8, 2, 1536)
            for k in range(1 if i == 0 else 0, PER_PLANE):
                peer = ep_peer((PLANES - offset_of(i)) % PLANES, k)
                remote(give.at[index_of(peer)], got.at[me], give_send, got_sem, peer).start()
        if b == 0:
            got[me] = give[me]

    def forwards(b):
        for i in range(4 * b, 4 * b + 4):
            forward(i)
            if i % 2 == 1:
                ring_step(i // 2 + 2)

    forwards(0)
    for load in loads:
        load.wait()
    forwards(1)
    expert_in(0)
    forwards(2)
    expert_out(0)
    expert_in(1)
    forwards(3)
    expert_out(1)
    expert_in(2)

    def columns(dx):
        return shared_w.at[:, ((x + 4 - dx) % 4) * 2 + c]

    def other_core(dx):
        return remote(columns(dx), columns(dx), wc_send, wc_sem.at[dx], ep_peer(0, 1))

    for n in (1, 2, 3):
        remote(columns(0), columns(0), wx_send, wx_sem.at[n - 1], ep_peer(0, 2 * n)).start()
    other_core(0).start()
    expert_in(3)
    expert_out(2)
    for n, d in enumerate(tps):
        remote(all_tokens.at[y], all_tokens.at[y], tok_send, tok_sem.at[n], tp_peer(d)).start()
    expert_out(3)
    for n in (1, 2, 3):
        drain(shared_w.at[:, 0], wx_sem.at[n - 1])
        other_core(n).start()

    for n in range(3):
        drain(all_tokens.at[0], tok_sem.at[n])
    square = jnp.zeros((128, 1), F32)
    for t in range(4):
        v = all_tokens[t].astype(F32)
        square += jnp.sum(v * v, axis=1, keepdims=True)
    scale = lax.rsqrt(square / 4096.0 + 1e-06)
    for t in range(4):
        v = all_tokens[t].astype(F32)
        mixed_in[:, t * 1024 : (t + 1) * 1024] = (v * scale * gain[t : t + 1, :]).astype(BF16)
    for n in range(4):
        drain(shared_w.at[:, 0], wc_sem.at[n])
    both = dot(mixed_in[...], shared_w[...].reshape(4096, 256))
    shared_hidden[y] = silu_mul(both[:, :128], both[:, 128:]).astype(BF16)
    for n, d in enumerate(tps):
        remote(shared_hidden.at[y], shared_hidden.at[y], sh_send, sh_sem.at[n], tp_peer(d)).start()

    token = expert
    first, second = ids[:, 0:1], ids[:, 1:2]
    names0, names1 = (lane == first).astype(F32), (lane == second).astype(F32)
    before = dot((lane < token).astype(BF16), (names0 + names1).astype(BF16))
    slot0 = jnp.sum(names0 * before, axis=1, keepdims=True).astype(jnp.int32)
    slot1 = jnp.sum(names1 * before, axis=1, keepdims=True).astype(jnp.int32)
    col = lax.broadcasted_iota(jnp.int32, (128, 256), 1)

    def weights(at, key0, key1):
        return jnp.where(at == key0, gates[:, 0:1], 0.0) + jnp.where(at == key1, gates[:, 1:2], 0.0)

    def parts_of(v):
        high = v.astype(BF16)
        return high, (v - high.astype(F32)).astype(BF16)

    pair = weights(
        col, jnp.where(slot0 < 2, 2 * first + slot0, -1), jnp.where(slot1 < 2, 2 * second + slot1, -1)
    )
    last = weights(col // 2, jnp.where(slot0 == 2, first, -1), jnp.where(slot1 == 2, second, -1))

    for n in range(3):
        drain(shared_hidden.at[0], sh_sem.at[n])
    full = jnp.concatenate([shared_hidden[t] for t in range(4)], axis=1)
    shared_out = dot(full, shared_down[...])

    drain(got.at[pl.ds(0, PEERS - 1)], got_sem)
    back = got[...].reshape(256, 1536)
    total = shared_out
    for part in parts_of(pair):
        total += dot(part, back[:, :1024])
    sides = []
    for p in (0, 1):
        side = jnp.zeros((128, 512), F32)
        for part in parts_of(jnp.where(col % 2 == p, last, 0.0)):
            side += dot(part, back[:, 1024:])
        sides.append(side)
    out[...] = (total + jnp.concatenate(sides, axis=1)).astype(BF16)

    drain(send.at[pl.ds(0, PEERS - 1)], send_sem)
    drain(rows.at[pl.ds(0, 3)], fwd_send)
    drain(hidden.at[pl.ds(0, 3)], hid_send)
    drain(give.at[pl.ds(0, PEERS - 1)], give_send)
    drain(all_tokens.at[pl.ds(0, 3)], tok_send)
    drain(shared_w.at[pl.ds(0, 15), 0], ring_send)
    drain(shared_w.at[:, pl.ds(0, 3)], wx_send)
    drain(shared_w.at[:, pl.ds(0, 4)], wc_send)
    drain(shared_hidden.at[pl.ds(0, 3)], sh_send)


def shards(
    tokens,
    norm_gain,
    expert_ids,
    expert_gates,
    gate_proj,
    up_proj,
    down_proj,
    shared_gate,
    shared_up,
    shared_down,
):
    vmem, hbm = pl.BlockSpec(memory_space=pltpu.VMEM), pl.BlockSpec(memory_space=pl.ANY)
    dma = pltpu.SemaphoreType.DMA
    return pl.pallas_call(
        layer_kernel,
        out_shape=jax.ShapeDtypeStruct(tokens.shape, BF16),
        in_specs=[vmem, vmem, vmem, vmem, vmem, hbm, hbm, hbm, vmem, vmem, hbm],
        out_specs=vmem,
        scratch_shapes=[
            pltpu.VMEM((128, 2, 1536), BF16),
            pltpu.VMEM((4, 128, 2, 1536), BF16),
            pltpu.VMEM((128, 4096), BF16),
            pltpu.VMEM((4, BATCHES, 128, 128), BF16),
            pltpu.VMEM((128, 2, 1536), BF16),
            pltpu.VMEM((128, 2, 1536), BF16),
            pltpu.VMEM((4, 128, 1024), BF16),
            pltpu.VMEM((16, 8, 32, 256), BF16),
            pltpu.VMEM((4, 128, 128), BF16),
            pltpu.VMEM((4096, 256), BF16),
            pltpu.VMEM((512, 1024), BF16),
            pltpu.VMEM((512, 1024), BF16),
            dma((4,)),
            dma,
            dma((16,)),
            dma,
            dma((3, 16)),
            dma,
            dma((3, BATCHES)),
            dma,
            dma,
            dma,
            dma((3,)),
            dma,
            dma((2, 8)),
            dma,
            dma((3,)),
            dma,
            dma((4,)),
            dma,
            dma((3,)),
        ],
        compiler_params=pltpu.CompilerParams(
            collective_id=0, has_side_effects=True, vmem_limit_bytes=60 * 2**20
        ),
    )(
        tokens,
        norm_gain.reshape(4, 1024),
        expert_ids,
        expert_ids.T,
        expert_gates,
        gate_proj,
        up_proj,
        down_proj,
        shared_gate,
        shared_up,
        shared_down,
    )


def solution(mesh):
    finer = Mesh(mesh.devices.reshape(16, 4, 2, mesh.shape["tp"]), (*EP, "tp"))
    in_specs = (
        P(EP, "tp"),
        P(),
        P(EP, None),
        P(EP, None),
        P(EP, None, "tp"),
        P(EP, None, "tp"),
        P(EP, None, "tp"),
        P(EP, "tp"),
        P(EP, "tp"),
        P(None, "tp"),
    )
    return jax.shard_map(
        shards, mesh=finer, in_specs=in_specs, out_specs=P(EP, "tp"), check_vma=False
    )
```

time: 274 us -> 136 us (0.50)
  Pallas kernels: 0 us -> 132 us
  waiting for transfers between devices: 107 us -> 0 us
  blocking collectives: 78.2 us -> 0 us
  starting transfers between devices: 28.6 us -> 0 us
  local copies, waits for them, and re-layouts: 31.8 us -> 4.5 us
  between operations: 13.7 us -> 0.01 us
  matrix products: 9.04 us -> 0 us
  other arithmetic: 4.13 us -> 0 us
    pallas_call x0 -> x1, Pallas kernels: none -> 132 us  [shards(): pl.pallas_call(layer_kernel, out_shape=jax.ShapeDtypeStruct(tokens.shape,...]
    all_to_all x3 -> x0, blocking collectives: 78.2 us -> none  [the longest x2 69.5 us: turned_blocks(): filled = lax.all_to_all(filled, axes[k], k, k, tiled=True)]
    all_gather x1 -> x0, waiting for transfers between devices: 67.5 us -> none  [sent_together(): filled, at, outs = (lax.all_gather(both, axis, axis=dim, tiled=True), 0, [])]
    all_to_all x4 -> x0, waiting for transfers between devices: 39.9 us -> none  [the longest x3 39.9 us: copy_for_each(): lax.all_to_all(jnp.broadcast_to(value[None], (peers, *value.shape)), axis...]
    all_to_all x4 -> x0, starting transfers between devices: 28.4 us -> none  [the longest x1 15.1 us: shards(): lax.all_to_all(expert_out, EP, split_axis=0, concat_axis=0, tiled=True)]
    dot_general x6 -> x0, matrix products: 9.04 us -> none  [the longest x1 3.01 us: shards(): jnp.einsum('secd,edh->sech', received, gate_proj, preferred_element_type=...]
    another operation x7 -> x0, local copies, waits for them, and re-layouts: 7.46 us -> none
    transpose x2 -> x0, local copies, waits for them, and re-layouts: 6.31 us -> none  [laid_out(): return jnp.moveaxis(blocks, 0, dim).reshape(shape)]
  transfers between devices with their start and end apart: 5 -> 0, of which waited for: 4 -> 0; matrix products, arithmetic and copies ran while one was open for 11% -> 0% of each run, Pallas kernels for 0% -> 0%
where the time goes in v2:
time: 136 us
  Pallas kernels  132 us (97%)
  local copies, waits for them, and re-layouts  4.5 us (3%)
    pallas_call x1, Pallas kernels, shards(): pl.pallas_call(layer_kernel, out_shape=jax.ShapeDtypeStruct(tokens.shape,...  132 us
    unnamed x7, local copies, waits for them, and re-layouts  3.16 us

profile of v2, /device:TPU:1, one launch (start us, length us, event | category | flops | bytes accessed | tf_op | source)
XLA Modules:
  0.0 136.2 jit_solution(16084407278075827280)
XLA Ops:
  0.0 0.0 copy-start.1
  0.0 1.3 reshape.3.gain
  1.3 0.0 copy-done.1
  1.4 0.0 copy-start
  1.4 0.7 copy.12.gates
  2.1 0.0 copy-done
  2.1 0.7 copy.11.ids
  2.8 131.7 %shard_map.100 = bf16[128,1024]{1,0:T(8,128)(2,1)} custom-call(bf16[128,1024]{1,0:T(8,128)(2,1)} %tokens.1, f32[4,1024]{1,0:T(4,128)} %reshape.3.gain, s32[128,2]{1,0:T(8,128)} %copy.11.ids, s32[2,128]{1,0:T(2,128)} %bitcast.1, f32[128,2]{1,0:T(8,128)} %copy.12.gates, bf16[1,4096,128]{2,1,0:T(8,128)(2,1)} %gate_hbm.1, bf16[1,4096,128]{2,1,0:T(8,128)(2,1)} %up_hbm.1, ...), custom_call_target="tpu_custom_call" | custom-call | tf_op jit(solution)/shard_map/pallas_call | solution.py:369
  134.5 1.7 %copy.14 = bf16[128,1024]{1,0:T(8,128)(2,1)} copy(bf16[128,1024]{1,0:T(8,128)(2,1)} %shard_map.100) | data formatting | bytes 524288
Async XLA Ops:
  0.0 1.3 copy-start.1
  1.4 0.7 copy-start

commit v3 on v2

--- a/solution.py
+++ b/solution.py
@@ -12,11 +12,18 @@
 F32 = jnp.float32
 PLANES, PER_PLANE, PEERS = 16, 8, 128
 BATCHES = 4
-
-
-def offset_of(i):
-    half = (i + 1) // 2
-    return (i % 2) * half + (1 - i % 2) * ((PLANES - half) % PLANES)
+NEAR = 4
+LAG = 2
+RELAYED = 0
+
+
+ORDER = (0, 1, 15, 2, 14, 3, 13, 4, 12, 5, 11, 6, 10, 7, 9, 8)
+SCHEDULE = (
+    "R1", "I8", "F0", "F1", "F2", "F3", "R2", "I12", "F4", "F5", "F6", "F7",
+    "R3", "I16", "E0", "F8", "F9", "D0", "F10", "F11", "R4", "E1", "F12", "F13",
+    "D1", "F14", "F15", "J0", "E2", "E3", "D2", "T0", "D3", "K0", "X0", "S0",
+    "S1",
+)
 
 
 def dot(a, b):
@@ -41,9 +48,8 @@
 def layer_kernel(
     tokens,
     gain,
-    ids,
     ids_t,
-    gates,
+    gates_t,
     gate_hbm,
     up_hbm,
     down_hbm,
@@ -60,6 +66,7 @@
     all_tokens,
     shared_w,
     shared_hidden,
+    normed,
     gate_up,
     down,
     shared_down,
@@ -76,6 +83,7 @@
     tok_sem,
     ring_send,
     ring_sem,
+    jump_sem,
     wx_send,
     wx_sem,
     wc_send,
@@ -112,12 +120,9 @@
 
     barrier = pltpu.get_barrier_semaphore()
 
-    def greet(f, _):
-        peer = ep_peer(offset_of(f // PER_PLANE), f % PER_PLANE)
-        pl.semaphore_signal(barrier, inc=1, device_id=peer, device_id_type=MESH)
-        return 0
-
-    lax.fori_loop(1, PEERS, greet, 0)
+    for dz in range(PLANES):
+        for k in range(0 if dz else 1, PER_PLANE):
+            pl.semaphore_signal(barrier, inc=1, device_id=ep_peer(dz, k), device_id_type=MESH)
     for d in tps:
         pl.semaphore_signal(barrier, inc=1, device_id=tp_peer(d), device_id_type=MESH)
 
@@ -155,15 +160,13 @@
     shared_w[z, w, :, :128] = shared_gate[...]
     shared_w[z, w, :, 128:] = shared_up[...]
 
-    pl.semaphore_wait(barrier, PEERS - 1 + 3)
-
-    def dispatch(f, _):
-        i = f // PER_PLANE
-        peer = ep_peer(offset_of(i), f % PER_PLANE)
-        remote(send.at[index_of(peer)], rows.at[y, me], send_sem, row_sem.at[i], peer).start()
-        return 0
-
-    lax.fori_loop(1, PEERS, dispatch, 0)
+    with jax.named_scope("barrier"):
+        pl.semaphore_wait(barrier, PEERS - 1 + 3)
+
+    def inject(i):
+        for k in range(0 if ORDER[i] else 1, PER_PLANE):
+            peer = ep_peer(ORDER[i], k)
+            remote(send.at[index_of(peer)], rows.at[y, me], send_sem, row_sem.at[i], peer).start()
 
     def ring(h, side):
         plane = (z + PLANES - (h - 1)) % PLANES if side == 0 else (z + h - 1) % PLANES
@@ -171,33 +174,64 @@
         peer = ep_peer(1 if side == 0 else PLANES - 1, 0)
         return remote(block, block, ring_send, ring_sem.at[side, h - 1], peer)
 
+    def spread(plane):
+        block = shared_w.at[plane, w]
+        for n in (1, 2, 3):
+            remote(block, block, wx_send, wx_sem.at[n - 1], ep_peer(0, 2 * n)).start()
+        remote(block, block, wc_send, wc_sem.at[0], ep_peer(0, 1)).start()
+
     def ring_step(h):
         for side in (0, 1):
-            if 1 < h and not (side == 1 and h - 1 > 7):
+            if h > 1:
                 ring(h - 1, side).wait_recv()
-            if h <= (8, 7)[side]:
+            if h <= NEAR:
                 ring(h, side).start()
-
-    ring_step(1)
+        if h == 1:
+            spread(z)
+        else:
+            for plane in ((z + PLANES - (h - 1)) % PLANES, (z + h - 1) % PLANES):
+                spread(plane)
+
+    def jump():
+        for far, first, last in ((NEAR, PLANES - NEAR, PLANES - 1), (PLANES - NEAR, 1, NEAR - 1)):
+            for dz in range(first, last + 1):
+                block = shared_w.at[(z + dz) % PLANES, w]
+                remote(block, block, ring_send, jump_sem, ep_peer(far, 0)).start()
+
+    def land():
+        drain(shared_w.at[pl.ds(0, 2 * NEAR - 1), 0], jump_sem)
+        for dz in range(NEAR + 1, PLANES - NEAR):
+            spread((z + dz) % PLANES)
 
     def plane_of(i):
-        return (z + PLANES - offset_of(i)) % PLANES
+        return (z + PLANES - ORDER[i]) % PLANES
 
     def forward(i):
         group = rows.at[y, pl.ds(plane_of(i) * PER_PLANE, PER_PLANE)]
-        if i == 0:
-            drain(rows.at[y, pl.ds(0, PER_PLANE - 1)], row_sem.at[0])
+        if ORDER[i] == 0:
+            drain(rows.at[y, pl.ds(0, PER_PLANE - 1)], row_sem.at[i])
         else:
             drain(group, row_sem.at[i])
-        for n, d in enumerate(tps):
+        for n, d in enumerate((1, 3) if i < RELAYED else (1, 3, 2)):
             remote(group, group, fwd_send, fwd_sem.at[n, i], tp_peer(d)).start()
 
+    def relay(i):
+        at = plane_of(i) * PER_PLANE
+        for n, d in enumerate((1, 3)):
+            source = (y + 4 - d) % 4
+            drain(rows.at[source, pl.ds(at, PER_PLANE)], fwd_sem.at[n, i])
+            half = rows.at[source, pl.ds(at + 4 * n, 4)]
+            remote(half, half, fwd_send, fwd_sem.at[2 + n, i], tp_peer(d)).start()
+
     even = parity((64, 512), 0) == 0
+
+    def gain_row(t):
+        return jnp.concatenate([gain[8 * t + n : 8 * t + n + 1, :] for n in range(8)], axis=1)
 
     def expert_in(b):
         for i in range(4 * b, 4 * b + 4):
-            for n in range(3):
-                drain(rows.at[0, pl.ds(0, PER_PLANE)], fwd_sem.at[n, i])
+            for n in (2, 3) if i < RELAYED else (0, 1, 2):
+                drain(rows.at[0, pl.ds(0, 4 if i < RELAYED else PER_PLANE)], fwd_sem.at[n, i])
 
         def batch(t):
             parts = [
@@ -218,7 +252,7 @@
         scale_last = lax.rsqrt(square_last / 4096.0 + 1e-06)
         for t in range(4):
             v = batch(t).astype(F32)
-            g = gain[t : t + 1, :]
+            g = gain_row(t)
             mixed_in[0:64, t * 1024 : (t + 1) * 1024] = (v[:, :1024] * scale_pair * g).astype(BF16)
             last = v[:, 1024:] * scale_last
             for p in (0, 1):
@@ -244,29 +278,11 @@
             i = 4 * b + j
             plane = plane_of(i)
             give[pl.ds(plane * PER_PLANE, PER_PLANE)] = res[16 * j : 16 * j + 16].reshape(8, 2, 1536)
-            for k in range(1 if i == 0 else 0, PER_PLANE):
-                peer = ep_peer((PLANES - offset_of(i)) % PLANES, k)
+            for k in range(0 if ORDER[i] else 1, PER_PLANE):
+                peer = ep_peer((PLANES - ORDER[i]) % PLANES, k)
                 remote(give.at[index_of(peer)], got.at[me], give_send, got_sem, peer).start()
-        if b == 0:
-            got[me] = give[me]
-
-    def forwards(b):
-        for i in range(4 * b, 4 * b + 4):
-            forward(i)
-            if i % 2 == 1:
-                ring_step(i // 2 + 2)
-
-    forwards(0)
-    for load in loads:
-        load.wait()
-    forwards(1)
-    expert_in(0)
-    forwards(2)
-    expert_out(0)
-    expert_in(1)
-    forwards(3)
-    expert_out(1)
-    expert_in(2)
+            if ORDER[i] == 0:
+                got[me] = give[me]
 
     def columns(dx):
         return shared_w.at[:, ((x + 4 - dx) % 4) * 2 + c]
@@ -274,37 +290,81 @@
     def other_core(dx):
         return remote(columns(dx), columns(dx), wc_send, wc_sem.at[dx], ep_peer(0, 1))
 
-    for n in (1, 2, 3):
-        remote(columns(0), columns(0), wx_send, wx_sem.at[n - 1], ep_peer(0, 2 * n)).start()
-    other_core(0).start()
-    expert_in(3)
-    expert_out(2)
-    for n, d in enumerate(tps):
-        remote(all_tokens.at[y], all_tokens.at[y], tok_send, tok_sem.at[n], tp_peer(d)).start()
-    expert_out(3)
-    for n in (1, 2, 3):
-        drain(shared_w.at[:, 0], wx_sem.at[n - 1])
-        other_core(n).start()
-
-    for n in range(3):
-        drain(all_tokens.at[0], tok_sem.at[n])
-    square = jnp.zeros((128, 1), F32)
-    for t in range(4):
-        v = all_tokens[t].astype(F32)
-        square += jnp.sum(v * v, axis=1, keepdims=True)
-    scale = lax.rsqrt(square / 4096.0 + 1e-06)
-    for t in range(4):
-        v = all_tokens[t].astype(F32)
-        mixed_in[:, t * 1024 : (t + 1) * 1024] = (v * scale * gain[t : t + 1, :]).astype(BF16)
-    for n in range(4):
-        drain(shared_w.at[:, 0], wc_sem.at[n])
-    both = dot(mixed_in[...], shared_w[...].reshape(4096, 256))
-    shared_hidden[y] = silu_mul(both[:, :128], both[:, 128:]).astype(BF16)
-    for n, d in enumerate(tps):
-        remote(shared_hidden.at[y], shared_hidden.at[y], sh_send, sh_sem.at[n], tp_peer(d)).start()
+    def pass_columns():
+        for n in (1, 2, 3):
+            drain(shared_w.at[:, 0], wx_sem.at[n - 1])
+            other_core(n).start()
+
+    def send_tokens():
+        for n, d in enumerate(tps):
+            remote(all_tokens.at[y], all_tokens.at[y], tok_send, tok_sem.at[n], tp_peer(d)).start()
+
+    def shared_norm():
+        for n in range(3):
+            drain(all_tokens.at[0], tok_sem.at[n])
+        square = jnp.zeros((128, 1), F32)
+        for t in range(4):
+            v = all_tokens[t].astype(F32)
+            square += jnp.sum(v * v, axis=1, keepdims=True)
+        scale = lax.rsqrt(square / 4096.0 + 1e-06)
+        for t in range(4):
+            v = all_tokens[t].astype(F32)
+            normed[:, t * 1024 : (t + 1) * 1024] = (v * scale * gain_row(t)).astype(BF16)
+
+    def shared_in():
+        for n in range(4):
+            drain(shared_w.at[:, 0], wc_sem.at[n])
+        both = dot(normed[...], shared_w[...].reshape(4096, 256))
+        shared_hidden[y] = silu_mul(both[:, :128], both[:, 128:]).astype(BF16)
+        for n, d in enumerate(tps):
+            remote(shared_hidden.at[y], shared_hidden.at[y], sh_send, sh_sem.at[n], tp_peer(d)).start()
+
+    loaded = False
+    injected, relayed = 0, 0
+    for step in SCHEDULE:
+        what, n = step[0], int(step[1:])
+        with jax.named_scope(step):
+            if what == "R":
+                ring_step(n)
+            elif what == "I":
+                while injected < n:
+                    inject(injected)
+                    injected += 1
+            elif what == "F":
+                forward(n)
+                while relayed <= min(n - LAG, RELAYED - 1):
+                    relay(relayed)
+                    relayed += 1
+            elif what == "E":
+                while relayed < min(4 * n + 4, RELAYED):
+                    relay(relayed)
+                    relayed += 1
+                if not loaded:
+                    for load in loads:
+                        load.wait()
+                    loaded = True
+                expert_in(n)
+            elif what == "D":
+                expert_out(n)
+            elif what == "T":
+                send_tokens()
+            elif what == "J":
+                ring_step(NEAR + 1)
+                jump()
+            elif what == "K":
+                land()
+            elif what == "X":
+                pass_columns()
+            elif what == "S":
+                (shared_norm, shared_in)[n]()
 
     token = expert
-    first, second = ids[:, 0:1], ids[:, 1:2]
+
+    def column(v):
+        return jnp.sum(jnp.where(token == lane, v, jnp.zeros_like(v)), axis=1, keepdims=True)
+
+    first, second = column(ids_t[0:1, :]), column(ids_t[1:2, :])
+    gate0, gate1 = column(gates_t[0:1, :]), column(gates_t[1:2, :])
     names0, names1 = (lane == first).astype(F32), (lane == second).astype(F32)
     before = dot((lane < token).astype(BF16), (names0 + names1).astype(BF16))
     slot0 = jnp.sum(names0 * before, axis=1, keepdims=True).astype(jnp.int32)
@@ -312,7 +372,7 @@
     col = lax.broadcasted_iota(jnp.int32, (128, 256), 1)
 
     def weights(at, key0, key1):
-        return jnp.where(at == key0, gates[:, 0:1], 0.0) + jnp.where(at == key1, gates[:, 1:2], 0.0)
+        return jnp.where(at == key0, gate0, 0.0) + jnp.where(at == key1, gate1, 0.0)
 
     def parts_of(v):
         high = v.astype(BF16)
@@ -323,12 +383,14 @@
     )
     last = weights(col // 2, jnp.where(slot0 == 2, first, -1), jnp.where(slot1 == 2, second, -1))
 
-    for n in range(3):
-        drain(shared_hidden.at[0], sh_sem.at[n])
+    with jax.named_scope("shwait"):
+        for n in range(3):
+            drain(shared_hidden.at[0], sh_sem.at[n])
     full = jnp.concatenate([shared_hidden[t] for t in range(4)], axis=1)
     shared_out = dot(full, shared_down[...])
 
-    drain(got.at[pl.ds(0, PEERS - 1)], got_sem)
+    with jax.named_scope("gotwait"):
+        drain(got.at[pl.ds(0, PEERS - 1)], got_sem)
     back = got[...].reshape(256, 1536)
     total = shared_out
     for part in parts_of(pair):
@@ -369,7 +431,7 @@
     return pl.pallas_call(
         layer_kernel,
         out_shape=jax.ShapeDtypeStruct(tokens.shape, BF16),
-        in_specs=[vmem, vmem, vmem, vmem, vmem, hbm, hbm, hbm, vmem, vmem, hbm],
+        in_specs=[vmem, vmem, vmem, vmem, hbm, hbm, hbm, vmem, vmem, hbm],
         out_specs=vmem,
         scratch_shapes=[
             pltpu.VMEM((128, 2, 1536), BF16),
@@ -381,6 +443,7 @@
             pltpu.VMEM((4, 128, 1024), BF16),
             pltpu.VMEM((16, 8, 32, 256), BF16),
             pltpu.VMEM((4, 128, 128), BF16),
+            pltpu.VMEM((128, 4096), BF16),
             pltpu.VMEM((4096, 256), BF16),
             pltpu.VMEM((512, 1024), BF16),
             pltpu.VMEM((512, 1024), BF16),
@@ -388,7 +451,7 @@
             dma,
             dma((16,)),
             dma,
-            dma((3, 16)),
+            dma((4, 16)),
             dma,
             dma((3, BATCHES)),
             dma,
@@ -396,7 +459,8 @@
             dma,
             dma((3,)),
             dma,
-            dma((2, 8)),
+            dma((2, NEAR)),
+            dma,
             dma,
             dma((3,)),
             dma,
@@ -409,10 +473,9 @@
         ),
     )(
         tokens,
-        norm_gain.reshape(4, 1024),
-        expert_ids,
+        norm_gain.reshape(32, 128),
         expert_ids.T,
-        expert_gates,
+        expert_gates.T,
         gate_proj,
         up_proj,
         down_proj,

time: 136 us -> 104 us (0.76)
  the two profiles are of different devices: /device:TPU:1 before, /device:TPU:449 now
where the time goes in v3:
time: 104 us
  Pallas kernels  102 us (98%)
  local copies, waits for them, and re-layouts  1.67 us (2%)
    pallas_call x1, Pallas kernels, shards(): pl.pallas_call(layer_kernel, out_shape=jax.ShapeDtypeStruct(tokens.shape,...  102 us

profile of v3, /device:TPU:449, one launch (start us, length us, event | category | flops | bytes accessed | tf_op | source)
XLA Modules:
  0.0 104.1 jit_solution(10348156447593382439)
XLA Ops:
  0.0 102.4 %shard_map.100 = bf16[128,1024]{1,0:T(8,128)(2,1)} custom-call(bf16[128,1024]{1,0:T(8,128)(2,1)} %tokens.1, f32[32,128]{1,0:T(8,128)} %bitcast.3, s32[2,128]{1,0:T(2,128)} %bitcast.4, f32[2,128]{1,0:T(2,128)} %bitcast.5, bf16[1,4096,128]{2,1,0:T(8,128)(2,1)} %gate_hbm.1, bf16[1,4096,128]{2,1,0:T(8,128)(2,1)} %up_hbm.1, bf16[1,512,1024]{2,1,0:T(8,128)(2,1)} %down_hbm.1, ...), custom_call_target="tpu_custom_call" | custom-call | tf_op jit(solution)/shard_map/pallas_call | solution.py:431
  102.5 1.7 %copy.12 = bf16[128,1024]{1,0:T(8,128)(2,1)} copy(bf16[128,1024]{1,0:T(8,128)(2,1)} %shard_map.100) | data formatting | bytes 524288

commit v4 on v3

--- a/solution.py
+++ b/solution.py
@@ -67,6 +67,7 @@
     shared_w,
     shared_hidden,
     normed,
+    total,
     gate_up,
     down,
     shared_down,
@@ -192,15 +193,14 @@
             for plane in ((z + PLANES - (h - 1)) % PLANES, (z + h - 1) % PLANES):
                 spread(plane)
 
-    def jump():
-        for far, first, last in ((NEAR, PLANES - NEAR, PLANES - 1), (PLANES - NEAR, 1, NEAR - 1)):
-            for dz in range(first, last + 1):
-                block = shared_w.at[(z + dz) % PLANES, w]
-                remote(block, block, ring_send, jump_sem, ep_peer(far, 0)).start()
-
-    def land():
-        drain(shared_w.at[pl.ds(0, 2 * NEAR - 1), 0], jump_sem)
-        for dz in range(NEAR + 1, PLANES - NEAR):
+    def jump(n, moves):
+        for far, dz in moves:
+            block = shared_w.at[(z + dz) % PLANES, w]
+            remote(block, block, ring_send, jump_sem.at[n], ep_peer(far, 0)).start()
+
+    def land(n, planes):
+        drain(shared_w.at[pl.ds(0, len(planes)), 0], jump_sem.at[n])
+        for dz in planes:
             spread((z + dz) % PLANES)
 
     def plane_of(i):
@@ -280,7 +280,7 @@
             give[pl.ds(plane * PER_PLANE, PER_PLANE)] = res[16 * j : 16 * j + 16].reshape(8, 2, 1536)
             for k in range(0 if ORDER[i] else 1, PER_PLANE):
                 peer = ep_peer((PLANES - ORDER[i]) % PLANES, k)
-                remote(give.at[index_of(peer)], got.at[me], give_send, got_sem, peer).start()
+                remote(give.at[index_of(peer)], got.at[me], give_send, got_sem.at[b], peer).start()
             if ORDER[i] == 0:
                 got[me] = give[me]
 
@@ -350,9 +350,9 @@
                 send_tokens()
             elif what == "J":
                 ring_step(NEAR + 1)
-                jump()
+                jump(0, ((4, 12), (4, 13), (4, 14), (4, 15), (12, 1), (12, 2), (12, 3)))
             elif what == "K":
-                land()
+                land(0, (5, 6, 7, 8, 9, 10, 11))
             elif what == "X":
                 pass_columns()
             elif what == "S":
@@ -369,7 +369,11 @@
     before = dot((lane < token).astype(BF16), (names0 + names1).astype(BF16))
     slot0 = jnp.sum(names0 * before, axis=1, keepdims=True).astype(jnp.int32)
     slot1 = jnp.sum(names1 * before, axis=1, keepdims=True).astype(jnp.int32)
-    col = lax.broadcasted_iota(jnp.int32, (128, 256), 1)
+    col = lax.broadcasted_iota(jnp.int32, (128, 64), 1)
+    pair0 = jnp.where(slot0 < 2, 2 * first + slot0, -1)
+    pair1 = jnp.where(slot1 < 2, 2 * second + slot1, -1)
+    last0 = jnp.where(slot0 == 2, first, -1)
+    last1 = jnp.where(slot1 == 2, second, -1)
 
     def weights(at, key0, key1):
         return jnp.where(at == key0, gate0, 0.0) + jnp.where(at == key1, gate1, 0.0)
@@ -378,30 +382,35 @@
         high = v.astype(BF16)
         return high, (v - high.astype(F32)).astype(BF16)
 
-    pair = weights(
-        col, jnp.where(slot0 < 2, 2 * first + slot0, -1), jnp.where(slot1 < 2, 2 * second + slot1, -1)
-    )
-    last = weights(col // 2, jnp.where(slot0 == 2, first, -1), jnp.where(slot1 == 2, second, -1))
+    def combine(b):
+        planes = [(z + ORDER[i]) % PLANES for i in range(4 * b, 4 * b + 4)]
+        at = col % 16
+        for j, plane in enumerate(planes):
+            at = jnp.where(col // 16 == j, at + plane * 16, at)
+        pair = parts_of(weights(at, pair0, pair1))
+        last = weights(at // 2, last0, last1)
+        sides = [parts_of(jnp.where(col % 2 == p, last, 0.0)) for p in (0, 1)]
+        own = 0 in ORDER[4 * b : 4 * b + 4]
+        drain(got.at[pl.ds(0, 4 * PER_PLANE - own)], got_sem.at[b])
+        back = jnp.concatenate(
+            [got[pl.ds(plane * PER_PLANE, PER_PLANE)].reshape(16, 1536) for plane in planes], axis=0
+        )
+        tail = back[:, 1024:]
+        return dot(pair[0], back[:, :1024]) + dot(pair[1], back[:, :1024]) + jnp.concatenate(
+            [dot(side[0], tail) + dot(side[1], tail) for side in sides], axis=1
+        )
 
     with jax.named_scope("shwait"):
         for n in range(3):
             drain(shared_hidden.at[0], sh_sem.at[n])
     full = jnp.concatenate([shared_hidden[t] for t in range(4)], axis=1)
-    shared_out = dot(full, shared_down[...])
-
-    with jax.named_scope("gotwait"):
-        drain(got.at[pl.ds(0, PEERS - 1)], got_sem)
-    back = got[...].reshape(256, 1536)
-    total = shared_out
-    for part in parts_of(pair):
-        total += dot(part, back[:, :1024])
-    sides = []
-    for p in (0, 1):
-        side = jnp.zeros((128, 512), F32)
-        for part in parts_of(jnp.where(col % 2 == p, last, 0.0)):
-            side += dot(part, back[:, 1024:])
-        sides.append(side)
-    out[...] = (total + jnp.concatenate(sides, axis=1)).astype(BF16)
+    total[...] = dot(full, shared_down[...])
+    for b in range(BATCHES):
+        with jax.named_scope(f"C{b}"):
+            if b < BATCHES - 1:
+                total[...] += combine(b)
+            else:
+                out[...] = (total[...] + combine(b)).astype(BF16)
 
     drain(send.at[pl.ds(0, PEERS - 1)], send_sem)
     drain(rows.at[pl.ds(0, 3)], fwd_send)
@@ -444,6 +453,7 @@
             pltpu.VMEM((16, 8, 32, 256), BF16),
             pltpu.VMEM((4, 128, 128), BF16),
             pltpu.VMEM((128, 4096), BF16),
+            pltpu.VMEM((128, 1024), F32),
             pltpu.VMEM((4096, 256), BF16),
             pltpu.VMEM((512, 1024), BF16),
             pltpu.VMEM((512, 1024), BF16),
@@ -455,12 +465,12 @@
             dma,
             dma((3, BATCHES)),
             dma,
-            dma,
+            dma((BATCHES,)),
             dma,
             dma((3,)),
             dma,
             dma((2, NEAR)),
-            dma,
+            dma((2,)),
             dma,
             dma((3,)),
             dma,

time: 104 us -> 104 us (level)
  no operation moved by 1% of the time
where the time goes in v4:
time: 104 us
  Pallas kernels  102 us (98%)
  local copies, waits for them, and re-layouts  1.67 us (2%)
    pallas_call x1, Pallas kernels, shards(): pl.pallas_call(layer_kernel, out_shape=jax.ShapeDtypeStruct(tokens.shape,...  102 us

profile of v4, /device:TPU:449, one launch (start us, length us, event | category | flops | bytes accessed | tf_op | source)
XLA Modules:
  0.0 103.9 jit_solution(9332392219441897454)
XLA Ops:
  0.0 102.2 %shard_map.100 = bf16[128,1024]{1,0:T(8,128)(2,1)} custom-call(bf16[128,1024]{1,0:T(8,128)(2,1)} %tokens.1, f32[32,128]{1,0:T(8,128)} %bitcast.3, s32[2,128]{1,0:T(2,128)} %bitcast.4, f32[2,128]{1,0:T(2,128)} %bitcast.5, bf16[1,4096,128]{2,1,0:T(8,128)(2,1)} %gate_hbm.1, bf16[1,4096,128]{2,1,0:T(8,128)(2,1)} %up_hbm.1, bf16[1,512,1024]{2,1,0:T(8,128)(2,1)} %down_hbm.1, ...), custom_call_target="tpu_custom_call" | custom-call | tf_op jit(solution)/shard_map/pallas_call | solution.py:440
  102.2 1.7 %copy.12 = bf16[128,1024]{1,0:T(8,128)(2,1)} copy(bf16[128,1024]{1,0:T(8,128)(2,1)} %shard_map.100) | data formatting | bytes 524288
